TPU v7x, 32 devices: a whole 2x2x4 slice. The times are simulated.
32 devices in a mesh: grp: 2 (over y), ep: 8 (over z, x), tp: 2 (over core).
Axes of the slice: x: 2, y: 2, z: 4, core: 2. Of those that a mesh axis runs over, the one named last changes fastest.
Arguments:
- fresh_inputs: bfloat16 [256, 2048], P(('grp', 'ep')), parts along dimension 0, may hold values from -6 to 6
- memory_arrays: float32 [256, 32, 64, 64], P(('grp', 'ep'), 'tp'), parts along dimension 0, may hold values from -4 to 4
- chosen_specialist: int32 [256, 2], P(('grp', 'ep')), parts along dimension 0, may hold values from 0 to 3, all different within a row; in each aligned block of 128 rows (0 to 127, 128 to 255, ...) at most 96 rows name the same one
- chosen_coefficient: bfloat16 [256, 2], P(('grp', 'ep')), parts along dimension 0, may hold values from 0.25 to 1
- first_rescale: float32 [2048], replicated, may hold values from 0.1 to 1.9
- second_rescale: float32 [2048], replicated, may hold values from 0.1 to 1.9
- receiver_projector: bfloat16 [2048, 2048], P('tp', 'ep'), may hold values from -0.125 to 0.125
- address_projector: bfloat16 [2048, 2048], P('tp', 'ep'), may hold values from -0.125 to 0.125
- content_projector: bfloat16 [2048, 2048], P('tp', 'ep'), may hold values from -0.125 to 0.125
- final_projector: bfloat16 [2048, 2048], P('tp', 'ep'), may hold values from -0.125 to 0.125
- forget_narrowing: bfloat16 [2048, 64], replicated, may hold values from -0.125 to 0.125
- forget_widening: bfloat16 [64, 2048], P(None, 'tp'), may hold values from -0.75 to 0.75
- forget_bias: float32 [2048], P('tp'), may hold values from -3 to 1
- learning_narrowing: bfloat16 [2048, 64], replicated, may hold values from -0.125 to 0.125
- learning_widening: bfloat16 [64, 2048], P(None, 'tp'), may hold values from -0.75 to 0.75
- learning_bias: float32 [2048], P('tp'), may hold values from -1.5 to 1.5
- lane_scaling: float32 [2048], P('tp'), may hold values from 0.1 to 1.9
- instant_reward: float32 [32, 64], P('tp'), may hold values from -0.5 to 0.5
- specialist_switch: bfloat16 [2048, 28672], P(None, ('ep', 'tp')), may hold values from -0.125 to 0.125
- specialist_expand: bfloat16 [2048, 28672], P(None, ('ep', 'tp')), may hold values from -0.125 to 0.125
- specialist_contract: bfloat16 [28672, 2048], P(('ep', 'tp')), may hold values from -0.0625 to 0.0625
- common_activator: bfloat16 [2048, 5632], P(None, ('ep', 'tp')), may hold values from -0.125 to 0.125
- common_expand: bfloat16 [2048, 5632], P(None, ('ep', 'tp')), may hold values from -0.125 to 0.125
- common_contract: bfloat16 [5632, 2048], P(('ep', 'tp')), may hold values from -0.078125 to 0.078125
- common_switch: bfloat16 [2048], replicated, may hold values from -0.125 to 0.125
Outputs:
- new_tokens: bfloat16 [256, 2048], P(('grp', 'ep', 'tp')), parts along dimension 0
- memory_after: float32 [256, 32, 64, 64], P(('grp', 'ep'), 'tp'), parts along dimension 0
There are 2 independent parts, one for each index of `grp`. A program takes and returns all parts, laid end to end along the dimension named above; an argument that names none is the same for every part. Nothing has to cross between parts.
Inputs may be any that keep to these rules, and one draw needn't show every extreme that they name: `chosen_specialist`: each row names 2 different experts. Over the whole batch no expert is named by more than 96 rows, and in every draw some expert is named by exactly 96 rows.
All inputs are finite; a program needn't handle non-finite values.
Results may differ from a plain program's by a relative error of at most 0.014.
Values may be sent and summed in bfloat16 or wider, within the bound.
A program may use at most 128 MiB of HBM per device.

v0:
```python
import jax
import jax.numpy as jnp
from jax import lax
from jax.sharding import PartitionSpec as P

LANE_WIDTH = 64
FF_E = 7168
RMS_EPS = 1e-06
GROUP_EPS = 0.00064
HIGHEST = lax.Precision.HIGHEST


def rms_norm(values, norm_gain):
    mean_sq = jnp.mean(values * values, axis=-1, keepdims=True)
    return values * lax.rsqrt(mean_sq + RMS_EPS) * norm_gain


def widen(rounded):
    return lax.optimization_barrier(rounded).astype(jnp.float32)


def evolve_memory(
    memory_arrays,
    receiver_lanes,
    address_lanes,
    content_lanes,
    forget_lanes,
    learning_lanes,
    lane_rescale,
    instant_reward,
):
    unit_key = address_lanes * lax.rsqrt(
        jnp.sum(address_lanes * address_lanes, axis=-1, keepdims=True) + 1.0
    )
    stepped_address = address_lanes * learning_lanes
    removal = jnp.einsum("bhvk,bhk->bhv", memory_arrays, unit_key, precision=HIGHEST)
    memory_after = (
        memory_arrays * forget_lanes[:, :, None, :]
        - removal[..., None] * (unit_key * learning_lanes)[:, :, None, :]
        + content_lanes[..., None] * stepped_address[:, :, None, :]
    )
    memory_retrieval = jnp.einsum("bhvk,bhk->bhv", memory_after, receiver_lanes, precision=HIGHEST)
    centred = memory_retrieval - jnp.mean(memory_retrieval, axis=-1, keepdims=True)
    unit_address = centred * lax.rsqrt(
        jnp.mean(centred * centred, axis=-1, keepdims=True) + GROUP_EPS
    )
    instant_extra = (
        jnp.sum(receiver_lanes * stepped_address * instant_reward, axis=-1, keepdims=True)
        * content_lanes
    )
    return (memory_after, unit_address * lane_rescale + instant_extra)


def swiglu(rows_in, gate_w, up_w):
    gate_val = jnp.dot(rows_in, gate_w, preferred_element_type=jnp.float32)
    up_val = jnp.dot(rows_in, up_w, preferred_element_type=jnp.float32)
    return (jax.nn.silu(gate_val) * up_val).astype(jnp.bfloat16)


def body(
    fresh_inputs,
    memory_arrays,
    chosen_specialist,
    chosen_coefficient,
    first_rescale,
    second_rescale,
    receiver_projector,
    address_projector,
    content_projector,
    final_projector,
    forget_narrowing,
    forget_widening,
    forget_bias,
    learning_narrowing,
    learning_widening,
    learning_bias,
    lane_scaling,
    instant_reward,
    specialist_switch,
    specialist_expand,
    specialist_contract,
    common_activator,
    common_expand,
    common_contract,
    common_switch,
):
    own_rows = fresh_inputs.shape[0]
    model_width = fresh_inputs.shape[1]
    tp_count = lax.axis_size("tp")
    tp_rank = lax.axis_index("tp")
    half_width = model_width // tp_count
    head_count = half_width // LANE_WIDTH
    residual = fresh_inputs.astype(jnp.float32)
    normed = rms_norm(residual, first_rescale).astype(jnp.bfloat16)
    normed_half = lax.dynamic_slice_in_dim(normed, tp_rank * half_width, half_width, 1)
    local_weights = jnp.stack((receiver_projector, address_projector, content_projector), axis=1)
    projected_rows = jnp.einsum(
        "rd,dkc->rkc",
        lax.all_gather(normed_half, "ep", axis=0, tiled=True),
        local_weights,
        preferred_element_type=jnp.float32,
    ).astype(jnp.bfloat16)
    partial_value = lax.all_to_all(projected_rows, "ep", split_axis=0, concat_axis=2, tiled=True)
    projected = lax.psum(widen(partial_value).astype(jnp.bfloat16), "tp")
    mine = lax.dynamic_slice_in_dim(projected, tp_rank * half_width, half_width, 2)

    def divide_lanes(channels):
        return channels.astype(jnp.float32).reshape(own_rows, head_count, LANE_WIDTH)

    decay_mid = jnp.tanh(
        jnp.dot(normed, forget_narrowing, preferred_element_type=jnp.float32)
    ).astype(jnp.bfloat16)
    decay_pre = forget_bias + jnp.dot(
        decay_mid, forget_widening, preferred_element_type=jnp.float32
    )
    decay_vals = jnp.exp(-jnp.exp(-jax.nn.softplus(-decay_pre) - 0.5))
    rate_mid = jnp.dot(normed, learning_narrowing, preferred_element_type=jnp.float32).astype(
        jnp.bfloat16
    )
    rate_vals = jax.nn.sigmoid(
        learning_bias + jnp.dot(rate_mid, learning_widening, preferred_element_type=jnp.float32)
    )
    memory_after, memory_retrieval = evolve_memory(
        memory_arrays,
        divide_lanes(mine[:, 0]),
        divide_lanes(mine[:, 1]),
        divide_lanes(mine[:, 2]),
        divide_lanes(decay_vals),
        divide_lanes(rate_vals),
        lane_scaling.reshape(head_count, LANE_WIDTH),
        instant_reward,
    )
    attended = memory_retrieval.reshape(own_rows, half_width).astype(jnp.bfloat16)
    done_rows = jnp.dot(
        lax.all_gather(attended, "ep", axis=0, tiled=True),
        final_projector,
        preferred_element_type=jnp.float32,
    ).astype(jnp.bfloat16)
    out_part = lax.all_to_all(done_rows, "ep", split_axis=0, concat_axis=1, tiled=True)
    mixed_out = lax.psum(widen(out_part).astype(jnp.bfloat16), "tp")
    residual = residual + mixed_out.astype(jnp.float32)
    ffn_in = rms_norm(residual, second_rescale).astype(jnp.bfloat16)
    all_in, all_weight, all_ids = (
        lax.all_gather(ffn_in, "ep", axis=0, tiled=True),
        lax.all_gather(chosen_coefficient, "ep", axis=0, tiled=True),
        lax.all_gather(chosen_specialist, "ep", axis=0, tiled=True),
    )
    column_count = specialist_switch.shape[1]
    flat_rank = lax.axis_index("ep") * tp_count + tp_rank
    expert = flat_rank * column_count // FF_E
    expert_share = jnp.sum(
        jnp.where(all_ids == expert, all_weight.astype(jnp.float32), 0.0), axis=1
    )
    hidden = swiglu(all_in, specialist_switch, specialist_expand)
    shared_hidden = swiglu(all_in, common_activator, common_expand)
    branch_scale = jax.nn.sigmoid(
        jnp.dot(all_in, common_switch, preferred_element_type=jnp.float32)
    )
    rows_mine = own_rows // tp_count
    expert_term = expert_share[:, None] * jnp.dot(
        hidden, specialist_contract, preferred_element_type=jnp.float32
    )
    routed = lax.psum_scatter(
        expert_term
        + branch_scale[:, None]
        * jnp.dot(shared_hidden, common_contract, preferred_element_type=jnp.float32),
        ("ep", "tp"),
        scatter_dimension=0,
        tiled=True,
    )
    own_residual = lax.dynamic_slice_in_dim(residual, tp_rank * rows_mine, rows_mine, 0)
    return ((own_residual + routed).astype(jnp.bfloat16), memory_after)


def solution(mesh):
    placed = (
        P(("grp", "ep"), None),
        P(("grp", "ep"), "tp", None, None),
        P(("grp", "ep"), None),
        P(("grp", "ep"), None),
        P(),
        P(),
        P("tp", "ep"),
        P("tp", "ep"),
        P("tp", "ep"),
        P("tp", "ep"),
        P(),
        P(None, "tp"),
        P("tp"),
        P(),
        P(None, "tp"),
        P("tp"),
        P("tp"),
        P("tp", None),
        P(None, ("ep", "tp")),
        P(None, ("ep", "tp")),
        P(("ep", "tp"), None),
        P(None, ("ep", "tp")),
        P(None, ("ep", "tp")),
        P(("ep", "tp"), None),
        P(),
    )
    return jax.shard_map(
        body,
        mesh=mesh,
        in_specs=placed,
        out_specs=(P(("grp", "ep", "tp"), None), P(("grp", "ep"), "tp", None, None)),
        check_vma=False,
    )
```

profile of v0, /device:TPU:0, one launch (start us, length us, event | category | flops | bytes accessed | tf_op | source)
XLA Modules:
  0.0 324.2 jit_solution(6716720031161532944)
XLA Ops:
  7.2 1.1 fusion.33
  9.3 32.6 %all_gather.15 = bf16[128,1024]{1,0:T(8,128)(2,1)S(1)} all-gather(bf16[16,1024]{1,0:T(8,128)(2,1)S(1)} %constant_dynamic-slice_fusion.1), channel_id=1, replica_groups=mesh['grp'=2,'ep'=8,'tp'=2] {'ep'}, dimensions={0}, use_global_device_ids=true | all-gather | bytes 294912 | tf_op jit(solution)/shard_map/all_gather | solution.py:99
  41.8 1.7 fusion.9
  44.5 5.5 %all-to-all-start = ((bf16[128,3,256]{2,1,0:T(4,128)(2,1)}), bf16[128,3,256]{2,1,0:T(4,128)(2,1)S(1)}, u32[]{:S(2)}, u32[]{:S(2)}) async-start(bf16[128,3,256]{2,1,0:T(4,128)(2,1)} %copy.30), calls=%async_computation | async-start | bytes 524288 | tf_op jit(solution)/shard_map/all_to_all | solution.py:103
  50.0 1.4 fusion.19
  51.5 6.7 %all-to-all-done = bf16[128,3,256]{2,1,0:T(4,128)(2,1)S(1)} async-done(((bf16[128,3,256]{2,1,0:T(4,128)(2,1)}), bf16[128,3,256]{2,1,0:T(4,128)(2,1)S(1)}, u32[]{:S(2)}, u32[]{:S(2)}) %all-to-all-start) | async-done | bytes 196640 | tf_op jit(solution)/shard_map/all_to_all | solution.py:103
  59.7 15.9 %all-reduce.3.cloned.1.call-done = bf16[16,3,2048]{2,0,1:T(8,128)(2,1)} async-done(((bf16[16,3,2048]{2,0,1:T(8,128)(2,1)}), bf16[16,3,2048]{2,0,1:T(8,128)(2,1)}) %all-reduce.3.cloned.1.call-update) | async-done | bytes 196624 | tf_op jit(solution)/shard_map/psum | solution.py:104
  77.1 15.4 %fusion.49 = f32[16,16,1,64]{3,2,1,0:T(1,128)S(1)} fusion(f32[16,16,64,1]{2,3,1,0:T(1,128)S(1)} %bitcast.75, f32[16,16,64,64]{3,2,1,0:T(8,128)} %param.26), kind=kOutput, calls=%fused_computation.80 | convolution fusion | flops 12582912 | bytes 4325376 | tf_op jit(solution)/shard_map/bhvk,bhk->bhv/dot_general | solution.py:36
  92.5 8.6 %multiply_add_fusion = f32[16,16,64,64]{3,2,1,0:T(8,128)S(1)} fusion(f32[16,16,64,64]{3,2,1,0:T(8,128)} %param.26, f32[16,16,64]{2,1,0:T(8,128)S(1)} %get-tuple-element.4, f32[16,16,64]{2,1,0:T(8,128)S(1)} %reshape.105, f32[16,16,64]{2,1,0:T(8,128)S(1)} %get-tuple-element.2, f32[16,16,64]{2,1,0:T(8,128)S(1)} %bitcast.74, f32[16,16,64]{2,1,0:T(8,128)S(1)} %mul.207), kind=kLoop, calls=%fused_computation.1 | loop fusion | flops 5242880 | bytes 8716288 | tf_op jit(solution)/shard_map/add | solution.py:38
  101.1 3.4 %copy-done.1 = f32[16,16,64,64]{3,2,1,0:T(8,128)} copy-done((f32[16,16,64,64]{3,2,1,0:T(8,128)}, f32[16,16,64,64]{3,2,1,0:T(8,128)S(1)}, u32[]{:S(2)}) %copy-start.1) | copy-done | bytes 4194328
  104.6 6.6 %fusion.50 = f32[16,16,1,64]{3,2,1,0:T(1,128)S(1)} fusion(f32[16,16,64,64]{3,2,1,0:T(8,128)S(1)} %multiply_add_fusion, bf16[16,16,64,1]{2,3,1,0:T(2,128)(2,1)S(1)} %reshape.124), kind=kOutput, calls=%fused_computation.81 | convolution fusion | flops 12582912 | bytes 4292608 | tf_op jit(solution)/shard_map/bhvk,bhk->bhv/dot_general | solution.py:42
  112.2 31.1 %all_gather.16 = bf16[128,1024]{1,0:T(8,128)(2,1)S(1)} all-gather(bf16[16,1024]{1,0:T(8,128)(2,1)S(1)} %convert_element_type.98), channel_id=1, replica_groups=mesh['grp'=2,'ep'=8,'tp'=2] {'ep'}, dimensions={0}, use_global_device_ids=true | all-gather | bytes 294912 | tf_op jit(solution)/shard_map/all_gather | solution.py:135
  144.1 5.4 %all-to-all-start.1 = ((bf16[8,16,256]{2,1,0:T(8,128)(2,1)}), bf16[8,16,256]{2,1,0:T(8,128)(2,1)S(1)}, u32[]{:S(2)}, u32[]{:S(2)}) async-start(bf16[8,16,256]{2,1,0:T(8,128)(2,1)} %bitcast.12), calls=%async_computation.1 | async-start | bytes 131072 | tf_op jit(solution)/shard_map/all_to_all | solution.py:139
  149.6 20.9 %all-gather.1 = bf16[8,16,2]{1,2,0:T(2,128)(2,1)S(1)} all-gather(bf16[1,16,2]{1,2,0:T(2,128)(2,1)S(1)} %bitcast.79), channel_id=1, replica_groups=mesh['grp'=2,'ep'=8,'tp'=2] {'ep'}, dimensions={0}, use_global_device_ids=true | all-gather | bytes 576 | tf_op jit(solution)/shard_map/all_gather | solution.py:145
  170.6 16.5 %all-gather = s32[8,16,2]{1,2,0:T(2,128)S(1)} all-gather(s32[1,16,2]{1,2,0:T(2,128)S(1)} %bitcast.78), channel_id=1, replica_groups=mesh['grp'=2,'ep'=8,'tp'=2] {'ep'}, dimensions={0}, use_global_device_ids=true | all-gather | bytes 1152 | tf_op jit(solution)/shard_map/all_gather | solution.py:146
  187.8 16.4 %all-reduce.5.cloned.1.call-done = bf16[16,2048]{1,0:T(8,128)(2,1)} async-done(((bf16[16,2048]{1,0:T(8,128)(2,1)}), bf16[16,2048]{1,0:T(8,128)(2,1)}) %all-reduce.5.cloned.1.call-update) | async-done | bytes 65552 | tf_op jit(solution)/shard_map/psum | solution.py:140
  204.2 1.0 convert_add_fusion
  206.1 31.8 %all_gather.19 = bf16[128,2048]{1,0:T(8,128)(2,1)S(1)} all-gather(bf16[16,2048]{1,0:T(8,128)(2,1)S(1)} %multiply_convert_fusion), channel_id=1, replica_groups=mesh['grp'=2,'ep'=8,'tp'=2] {'ep'}, dimensions={0}, use_global_device_ids=true | all-gather | bytes 589824 | tf_op jit(solution)/shard_map/all_gather | solution.py:144
  237.9 5.3 %fusion.51 = f32[128,1792]{1,0:T(8,128)} fusion(bf16[128,2048]{1,0:T(8,128)(2,1)S(1)} %all_gather.19, bf16[2048,1792]{1,0:T(8,128)(2,1)} %param.43), kind=kOutput, calls=%fused_computation.82 | convolution fusion | flops 939524096 | bytes 8781824 | tf_op jit(solution)/shard_map/dot_general | solution.py:55
  243.2 1.2 fusion.52
  244.7 9.1 %convolution_multiply_fusion.1 = f32[128,2048]{1,0:T(8,128)} fusion(bf16[1792,2048]{1,0:T(8,128)(2,1)} %param.45, bf16[128,2048]{1,0:T(8,128)(2,1)S(1)} %all_gather.19, bf16[2048,1792]{1,0:T(8,128)(2,1)} %param.44, f32[128,1792]{1,0:T(8,128)} %fusion.51, f32[128]{0:T(128)S(1)} %reshape.115), kind=kOutput, calls=%fused_computation.3 | convolution fusion | flops 1880686592 | bytes 17170944 | tf_op jit(solution)/shard_map/dot_general | solution.py:160
  253.7 3.8 %fusion.1 = f32[128,2048]{1,0:T(8,128)} fusion(f32[128,2048]{1,0:T(8,128)} %convolution_multiply_fusion.1, bf16[352,2048]{1,0:T(8,128)(2,1)S(1)} %copy-done, bf16[128,2048]{1,0:T(8,128)(2,1)S(1)} %all_gather.19, bf16[2048,352]{0,1:T(8,128)(2,1)S(1)} %copy-done.3, f32[128]{0:T(128)S(1)} %fusion.25, f32[128,352]{0,1:T(8,128)} %fusion.52), kind=kOutput, calls=%fused_computation.5 | convolution fusion | flops 369893376 | bytes 5685760 | tf_op jit(solution)/shard_map/dot_general | solution.py:166
  257.6 58.6 %reduce-scatter.2.cloned.1.call-done = f32[8,2048]{1,0:T(8,128)} async-done(((f32[128,2048]{1,0:T(8,128)}), f32[8,2048]{1,0:T(8,128)}) %reduce-scatter.2.cloned.1.call-update) | async-done | bytes 65552 | tf_op jit(solution)/shard_map/reduce_scatter | solution.py:163
  316.2 1.5 add_convert_fusion
  (68 shorter events, 8.7 us)
Async XLA Ops:
  7.2 246.6 %copy-start = (bf16[352,2048]{1,0:T(8,128)(2,1)S(1)}, bf16[352,2048]{1,0:T(8,128)(2,1)}, u32[]{:S(2)}) copy-start(bf16[352,2048]{1,0:T(8,128)(2,1)} %param.48) | copy-start | bytes 4325380
  7.2 52.0 %copy-start.6 = (bf16[2048,64]{0,1:T(8,128)(2,1)S(1)}, bf16[2048,64]{0,1:T(8,128)(2,1)}, u32[]{:S(2)}) copy-start(bf16[2048,64]{0,1:T(8,128)(2,1)} %param.35) | copy-start | bytes 786436
  7.2 52.0 %copy-start.7 = (bf16[64,1024]{1,0:T(8,128)(2,1)S(1)}, bf16[64,1024]{1,0:T(8,128)(2,1)}, u32[]{:S(2)}) copy-start(bf16[64,1024]{1,0:T(8,128)(2,1)} %param.36) | copy-start | bytes 393220
  7.2 52.0 %copy-start.10 = (f32[1024]{0:T(1024)S(1)}, f32[1024]{0:T(1024)}, u32[]{:S(2)}) copy-start(f32[1024]{0:T(1024)} %param.37) | copy-start | bytes 12292
  7.2 52.5 %copy-start.11 = (f32[1024]{0:T(1024)S(1)}, f32[1024]{0:T(1024)}, u32[]{:S(2)}) copy-start(f32[1024]{0:T(1024)} %param.41) | copy-start | bytes 12292
  44.5 13.7 %all-to-all-start = ((bf16[128,3,256]{2,1,0:T(4,128)(2,1)}), bf16[128,3,256]{2,1,0:T(4,128)(2,1)S(1)}, u32[]{:S(2)}, u32[]{:S(2)}) async-start(bf16[128,3,256]{2,1,0:T(4,128)(2,1)} %copy.30), calls=%async_computation | async-start | bytes 524288 | tf_op jit(solution)/shard_map/all_to_all | solution.py:103
  50.0 25.7 %all-reduce.3.cloned.1.call-start = ((), (), s32[]{:S(2)}) async-start(), calls=%async_computation.3 | async-start | bytes 393216 | tf_op jit(solution)/shard_map/psum | solution.py:104
  101.1 3.4 %copy-start.1 = (f32[16,16,64,64]{3,2,1,0:T(8,128)}, f32[16,16,64,64]{3,2,1,0:T(8,128)S(1)}, u32[]{:S(2)}) copy-start(f32[16,16,64,64]{3,2,1,0:T(8,128)S(1)} %multiply_add_fusion) | copy-start | bytes 12582916
  104.5 7.0 %copy-start.8 = (f32[16,64]{1,0:T(8,128)S(1)}, f32[16,64]{1,0:T(8,128)}, u32[]{:S(2)}) copy-start(f32[16,64]{1,0:T(8,128)} %param.42) | copy-start | bytes 12292
  104.5 38.8 %copy-start.5 = (bf16[1024,256]{1,0:T(8,128)(2,1)S(1)}, bf16[1024,256]{1,0:T(8,128)(2,1)}, u32[]{:S(2)}) copy-start(bf16[1024,256]{1,0:T(8,128)(2,1)} %param.34) | copy-start | bytes 1572868
  104.5 45.1 %copy-start.14 = (bf16[16,2]{0,1:T(2,128)(2,1)S(1)}, bf16[16,2]{0,1:T(2,128)(2,1)}, u32[]{:S(2)}) copy-start(bf16[16,2]{0,1:T(2,128)(2,1)} %param.28) | copy-start | bytes 196
  104.5 66.0 %copy-start.13 = (s32[16,2]{0,1:T(2,128)S(1)}, s32[16,2]{0,1:T(2,128)}, u32[]{:S(2)}) copy-start(s32[16,2]{0,1:T(2,128)} %param.27) | copy-start | bytes 388
  104.5 83.3 %copy-start.12 = (bf16[2048]{0:T(1024)(128)(2,1)S(1)}, bf16[2048]{0:T(1024)(128)(2,1)}, u32[]{:S(2)}) copy-start(bf16[2048]{0:T(1024)(128)(2,1)} %param.49) | copy-start | bytes 12292
  104.5 99.7 %copy-start.4 = (bf16[16,2048]{1,0:T(8,128)(2,1)S(1)}, bf16[16,2048]{1,0:T(8,128)(2,1)}, u32[]{:S(2)}) copy-start(bf16[16,2048]{1,0:T(8,128)(2,1)} %param.25) | copy-start | bytes 196612
  104.5 100.7 %copy-start.9 = (f32[2048]{0:T(1024)S(1)}, f32[2048]{0:T(1024)}, u32[]{:S(2)}) copy-start(f32[2048]{0:T(1024)} %param.30) | copy-start | bytes 24580
  144.1 42.9 %all-to-all-start.1 = ((bf16[8,16,256]{2,1,0:T(8,128)(2,1)}), bf16[8,16,256]{2,1,0:T(8,128)(2,1)S(1)}, u32[]{:S(2)}, u32[]{:S(2)}) async-start(bf16[8,16,256]{2,1,0:T(8,128)(2,1)} %bitcast.12), calls=%async_computation.1 | async-start | bytes 131072 | tf_op jit(solution)/shard_map/all_to_all | solution.py:139
  149.6 54.7 %all-reduce.5.cloned.1.call-start = ((), (), s32[]{:S(2)}) async-start(), calls=%async_computation.4 | async-start | bytes 131072 | tf_op jit(solution)/shard_map/psum | solution.py:140
  187.7 128.5 %reduce-scatter.2.cloned.1.call-start = ((), (), s32[]{:S(2)}) async-start(), calls=%async_computation.5 | async-start | bytes 1114112 | tf_op jit(solution)/shard_map/reduce_scatter | solution.py:163
  237.9 5.3 %copy-start.2 = (bf16[2048,352]{0,1:T(8,128)(2,1)S(1)}, bf16[2048,352]{0,1:T(8,128)(2,1)}, u32[]{:S(2)}) copy-start(bf16[2048,352]{0,1:T(8,128)(2,1)} %param.46) | copy-start | bytes 4325380
  244.7 9.1 %copy-start.3 = (bf16[2048,352]{0,1:T(8,128)(2,1)S(1)}, bf16[2048,352]{0,1:T(8,128)(2,1)}, u32[]{:S(2)}) copy-start(bf16[2048,352]{0,1:T(8,128)(2,1)} %param.47) | copy-start | bytes 4325380
Sparse Core Ops, SparseCore 0:
  59.3 16.3 all-reduce.2
  187.8 16.3 all-reduce.4
  257.7 58.4 reduce-scatter.1
where the time goes:
time: 325 us; the launch traced here: 324 us
  blocking collectives  133 us (41%)
  waiting for transfers between devices  97.7 us (30%)
  matrix products  46 us (14%)
  other arithmetic  15.8 us (5%)
  between operations  14.1 us (4%)
  starting transfers between devices  11.1 us (3%)
  local copies, waits for them, and re-layouts  6.74 us (2%)
    reduce_scatter x1, waiting for transfers between devices, body(): lax.psum_scatter(expert_term + branch_scale[:, None] * jnp.dot(shared_hid...  58.6 us
    all_gather x1, blocking collectives, body(): lax.all_gather(normed_half, 'ep', axis=0, tiled=True)  32.6 us
    all_gather x1, blocking collectives, body(): lax.all_gather(ffn_in, 'ep', axis=0, tiled=True)  31.8 us
    all_gather x1, blocking collectives, body(): lax.all_gather(attended, 'ep', axis=0, tiled=True)  31.1 us
    all_gather x1, blocking collectives, body(): lax.all_gather(chosen_coefficient, 'ep', axis=0, tiled=True)  20.9 us
    all_gather x1, blocking collectives, body(): lax.all_gather(chosen_specialist, 'ep', axis=0, tiled=True)  16.5 us
    psum x1, waiting for transfers between devices, body(): mixed_out = lax.psum(widen(out_part).astype(jnp.bfloat16), 'tp')  16.4 us
    psum x1, waiting for transfers between devices, body(): projected = lax.psum(widen(partial_value).astype(jnp.bfloat16), 'tp')  15.9 us
  transfers between devices with their start and end apart: 5, of which 4 were waited for; matrix products, arithmetic and copies ran while one was open for 1% of the time, Pallas kernels for 0%

commit v1 on v0

--- a/solution.py
+++ b/solution.py
@@ -137,7 +137,7 @@
         preferred_element_type=jnp.float32,
     ).astype(jnp.bfloat16)
     out_part = lax.all_to_all(done_rows, "ep", split_axis=0, concat_axis=1, tiled=True)
-    mixed_out = lax.psum(widen(out_part).astype(jnp.bfloat16), "tp")
+    mixed_out = jnp.sum(lax.all_gather(widen(out_part).astype(jnp.bfloat16), "tp"), axis=0)
     residual = residual + mixed_out.astype(jnp.float32)
     ffn_in = rms_norm(residual, second_rescale).astype(jnp.bfloat16)
     all_in, all_weight, all_ids = (

time: 325 us -> 306 us (0.942)
  waiting for transfers between devices: 97.7 us -> 79.4 us
    psum x1 -> x0, waiting for transfers between devices: 16.4 us -> none  [body(): mixed_out = lax.psum(widen(out_part).astype(jnp.bfloat16), 'tp')]
  transfers between devices with their start and end apart: 5 -> 4, of which waited for: 4 -> 3; matrix products, arithmetic and copies ran while one was open for 1% -> 1% of each run, Pallas kernels for 0% -> 0%
where the time goes in v1:
time: 306 us; the launch traced here: 305 us
  blocking collectives  134 us (44%)
  waiting for transfers between devices  79.4 us (26%)
  matrix products  46 us (15%)
  between operations  14.4 us (5%)
  other arithmetic  14.2 us (5%)
  starting transfers between devices  11 us (4%)
  local copies, waits for them, and re-layouts  6.13 us (2%)
    reduce_scatter x1, waiting for transfers between devices, body(): lax.psum_scatter(expert_term + branch_scale[:, None] * jnp.dot(shared_hid...  56.8 us
    all_gather x1, blocking collectives, body(): lax.all_gather(normed_half, 'ep', axis=0, tiled=True)  32.6 us
    all_gather x1, blocking collectives, body(): lax.all_gather(ffn_in, 'ep', axis=0, tiled=True)  31.3 us
    all_gather x1, blocking collectives, body(): lax.all_gather(attended, 'ep', axis=0, tiled=True)  31.1 us
    all_gather x1, blocking collectives, body(): lax.all_gather(chosen_coefficient, 'ep', axis=0, tiled=True)  20.9 us
    all_gather x1, blocking collectives, body(): lax.all_gather(chosen_specialist, 'ep', axis=0, tiled=True)  16.5 us
    psum x1, waiting for transfers between devices, body(): projected = lax.psum(widen(partial_value).astype(jnp.bfloat16), 'tp')  15.9 us
    dot_general x1, matrix products, evolve_memory(): jnp.einsum('bhvk,bhk->bhv', memory_arrays, unit_key, precision=HIGHEST)  15.4 us
  transfers between devices with their start and end apart: 4, of which 3 were waited for; matrix products, arithmetic and copies ran while one was open for 1% of the time, Pallas kernels for 0%

profile of v1, /device:TPU:0, one launch (start us, length us, event | category | flops | bytes accessed | tf_op | source)
XLA Modules:
  0.0 305.4 jit_solution(11259267874771029587)
XLA Ops:
  7.2 1.1 fusion.33
  8.3 0.9 fusion.35
  9.3 32.6 %all_gather.21 = bf16[128,1024]{1,0:T(8,128)(2,1)S(1)} all-gather(bf16[16,1024]{1,0:T(8,128)(2,1)S(1)} %constant_dynamic-slice_fusion.1), channel_id=1, replica_groups=mesh['grp'=2,'ep'=8,'tp'=2] {'ep'}, dimensions={0}, use_global_device_ids=true | all-gather | bytes 294912 | tf_op jit(solution)/shard_map/all_gather | solution.py:99
  41.8 1.7 fusion.9
  44.5 5.5 %all-to-all-start = ((bf16[128,3,256]{2,1,0:T(4,128)(2,1)}), bf16[128,3,256]{2,1,0:T(4,128)(2,1)S(1)}, u32[]{:S(2)}, u32[]{:S(2)}) async-start(bf16[128,3,256]{2,1,0:T(4,128)(2,1)} %copy.29), calls=%async_computation | async-start | bytes 524288 | tf_op jit(solution)/shard_map/all_to_all | solution.py:103
  50.0 1.4 fusion.19
  51.5 6.7 %all-to-all-done = bf16[128,3,256]{2,1,0:T(4,128)(2,1)S(1)} async-done(((bf16[128,3,256]{2,1,0:T(4,128)(2,1)}), bf16[128,3,256]{2,1,0:T(4,128)(2,1)S(1)}, u32[]{:S(2)}, u32[]{:S(2)}) %all-to-all-start) | async-done | bytes 196640 | tf_op jit(solution)/shard_map/all_to_all | solution.py:103
  59.7 15.9 %all-reduce.2.cloned.1.call-done = bf16[16,3,2048]{2,0,1:T(8,128)(2,1)} async-done(((bf16[16,3,2048]{2,0,1:T(8,128)(2,1)}), bf16[16,3,2048]{2,0,1:T(8,128)(2,1)}) %all-reduce.2.cloned.1.call-update) | async-done | bytes 196624 | tf_op jit(solution)/shard_map/psum | solution.py:104
  77.1 15.4 %fusion.49 = f32[16,16,1,64]{3,2,1,0:T(1,128)S(1)} fusion(f32[16,16,64,1]{2,3,1,0:T(1,128)S(1)} %bitcast.76, f32[16,16,64,64]{3,2,1,0:T(8,128)} %param.26), kind=kOutput, calls=%fused_computation.80 | convolution fusion | flops 12582912 | bytes 4325376 | tf_op jit(solution)/shard_map/bhvk,bhk->bhv/dot_general | solution.py:36
  92.5 8.6 %multiply_add_fusion = f32[16,16,64,64]{3,2,1,0:T(8,128)S(1)} fusion(f32[16,16,64,64]{3,2,1,0:T(8,128)} %param.26, f32[16,16,64]{2,1,0:T(8,128)S(1)} %get-tuple-element.4, f32[16,16,64]{2,1,0:T(8,128)S(1)} %reshape.105, f32[16,16,64]{2,1,0:T(8,128)S(1)} %get-tuple-element.2, f32[16,16,64]{2,1,0:T(8,128)S(1)} %bitcast.75, f32[16,16,64]{2,1,0:T(8,128)S(1)} %mul.207), kind=kLoop, calls=%fused_computation.1 | loop fusion | flops 5242880 | bytes 8716288 | tf_op jit(solution)/shard_map/add | solution.py:38
  101.1 3.4 %copy-done.1 = f32[16,16,64,64]{3,2,1,0:T(8,128)} copy-done((f32[16,16,64,64]{3,2,1,0:T(8,128)}, f32[16,16,64,64]{3,2,1,0:T(8,128)S(1)}, u32[]{:S(2)}) %copy-start.1) | copy-done | bytes 4194328
  104.6 6.6 %fusion.50 = f32[16,16,1,64]{3,2,1,0:T(1,128)S(1)} fusion(f32[16,16,64,64]{3,2,1,0:T(8,128)S(1)} %multiply_add_fusion, bf16[16,16,64,1]{2,3,1,0:T(2,128)(2,1)S(1)} %reshape.125), kind=kOutput, calls=%fused_computation.81 | convolution fusion | flops 12582912 | bytes 4292608 | tf_op jit(solution)/shard_map/bhvk,bhk->bhv/dot_general | solution.py:42
  112.2 31.1 %all_gather.22 = bf16[128,1024]{1,0:T(8,128)(2,1)S(1)} all-gather(bf16[16,1024]{1,0:T(8,128)(2,1)S(1)} %convert_element_type.100), channel_id=1, replica_groups=mesh['grp'=2,'ep'=8,'tp'=2] {'ep'}, dimensions={0}, use_global_device_ids=true | all-gather | bytes 294912 | tf_op jit(solution)/shard_map/all_gather | solution.py:135
  144.1 5.4 %all-to-all-start.1 = ((bf16[8,16,256]{2,1,0:T(8,128)(2,1)}), bf16[8,16,256]{2,1,0:T(8,128)(2,1)S(1)}, u32[]{:S(2)}, u32[]{:S(2)}) async-start(bf16[8,16,256]{2,1,0:T(8,128)(2,1)} %bitcast.12), calls=%async_computation.1 | async-start | bytes 131072 | tf_op jit(solution)/shard_map/all_to_all | solution.py:139
  149.6 20.9 %all-gather.2 = bf16[8,16,2]{1,2,0:T(2,128)(2,1)S(1)} all-gather(bf16[1,16,2]{1,2,0:T(2,128)(2,1)S(1)} %bitcast.81), channel_id=1, replica_groups=mesh['grp'=2,'ep'=8,'tp'=2] {'ep'}, dimensions={0}, use_global_device_ids=true | all-gather | bytes 576 | tf_op jit(solution)/shard_map/all_gather | solution.py:145
  170.6 16.5 %all-gather.1 = s32[8,16,2]{1,2,0:T(2,128)S(1)} all-gather(s32[1,16,2]{1,2,0:T(2,128)S(1)} %bitcast.80), channel_id=1, replica_groups=mesh['grp'=2,'ep'=8,'tp'=2] {'ep'}, dimensions={0}, use_global_device_ids=true | all-gather | bytes 1152 | tf_op jit(solution)/shard_map/all_gather | solution.py:146
  187.2 1.9 all-gather
  189.3 31.3 %all_gather.27 = bf16[128,2048]{1,0:T(8,128)(2,1)S(1)} all-gather(bf16[16,2048]{1,0:T(8,128)(2,1)S(1)} %multiply_convert_fusion), channel_id=1, replica_groups=mesh['grp'=2,'ep'=8,'tp'=2] {'ep'}, dimensions={0}, use_global_device_ids=true | all-gather | bytes 589824 | tf_op jit(solution)/shard_map/all_gather | solution.py:144
  220.7 5.3 %fusion.51 = f32[128,1792]{1,0:T(8,128)} fusion(bf16[128,2048]{1,0:T(8,128)(2,1)S(1)} %all_gather.27, bf16[2048,1792]{1,0:T(8,128)(2,1)} %param.43), kind=kOutput, calls=%fused_computation.82 | convolution fusion | flops 939524096 | bytes 8781824 | tf_op jit(solution)/shard_map/dot_general | solution.py:55
  226.0 1.2 fusion.52
  227.4 9.1 %convolution_multiply_fusion.1 = f32[128,2048]{1,0:T(8,128)} fusion(bf16[1792,2048]{1,0:T(8,128)(2,1)} %param.45, bf16[128,2048]{1,0:T(8,128)(2,1)S(1)} %all_gather.27, bf16[2048,1792]{1,0:T(8,128)(2,1)} %param.44, f32[128,1792]{1,0:T(8,128)} %fusion.51, f32[128]{0:T(128)S(1)} %reshape.116), kind=kOutput, calls=%fused_computation.3 | convolution fusion | flops 1880686592 | bytes 17170944 | tf_op jit(solution)/shard_map/dot_general | solution.py:160
  236.5 3.8 %fusion.1 = f32[128,2048]{1,0:T(8,128)} fusion(f32[128,2048]{1,0:T(8,128)} %convolution_multiply_fusion.1, bf16[352,2048]{1,0:T(8,128)(2,1)S(1)} %copy-done, bf16[128,2048]{1,0:T(8,128)(2,1)S(1)} %all_gather.27, bf16[2048,352]{0,1:T(8,128)(2,1)S(1)} %copy-done.3, f32[128]{0:T(128)S(1)} %fusion.25, f32[128,352]{0,1:T(8,128)} %fusion.52), kind=kOutput, calls=%fused_computation.5 | convolution fusion | flops 369893376 | bytes 5685760 | tf_op jit(solution)/shard_map/dot_general | solution.py:166
  240.3 56.8 %reduce-scatter.2.cloned.1.call-done = f32[8,2048]{1,0:T(8,128)} async-done(((f32[128,2048]{1,0:T(8,128)}), f32[8,2048]{1,0:T(8,128)}) %reduce-scatter.2.cloned.1.call-update) | async-done | bytes 65552 | tf_op jit(solution)/shard_map/reduce_scatter | solution.py:163
  297.1 1.5 add_convert_fusion
  (67 shorter events, 6.5 us)
Async XLA Ops:
  7.2 229.3 %copy-start = (bf16[352,2048]{1,0:T(8,128)(2,1)S(1)}, bf16[352,2048]{1,0:T(8,128)(2,1)}, u32[]{:S(2)}) copy-start(bf16[352,2048]{1,0:T(8,128)(2,1)} %param.48) | copy-start | bytes 4325380
  7.2 52.0 %copy-start.6 = (bf16[2048,64]{0,1:T(8,128)(2,1)S(1)}, bf16[2048,64]{0,1:T(8,128)(2,1)}, u32[]{:S(2)}) copy-start(bf16[2048,64]{0,1:T(8,128)(2,1)} %param.35) | copy-start | bytes 786436
  7.2 52.0 %copy-start.7 = (bf16[64,1024]{1,0:T(8,128)(2,1)S(1)}, bf16[64,1024]{1,0:T(8,128)(2,1)}, u32[]{:S(2)}) copy-start(bf16[64,1024]{1,0:T(8,128)(2,1)} %param.36) | copy-start | bytes 393220
  7.2 52.0 %copy-start.10 = (f32[1024]{0:T(1024)S(1)}, f32[1024]{0:T(1024)}, u32[]{:S(2)}) copy-start(f32[1024]{0:T(1024)} %param.37) | copy-start | bytes 12292
  7.2 52.5 %copy-start.11 = (f32[1024]{0:T(1024)S(1)}, f32[1024]{0:T(1024)}, u32[]{:S(2)}) copy-start(f32[1024]{0:T(1024)} %param.41) | copy-start | bytes 12292
  44.5 13.7 %all-to-all-start = ((bf16[128,3,256]{2,1,0:T(4,128)(2,1)}), bf16[128,3,256]{2,1,0:T(4,128)(2,1)S(1)}, u32[]{:S(2)}, u32[]{:S(2)}) async-start(bf16[128,3,256]{2,1,0:T(4,128)(2,1)} %copy.29), calls=%async_computation | async-start | bytes 524288 | tf_op jit(solution)/shard_map/all_to_all | solution.py:103
  50.0 25.7 %all-reduce.2.cloned.1.call-start = ((), (), s32[]{:S(2)}) async-start(), calls=%async_computation.3 | async-start | bytes 393216 | tf_op jit(solution)/shard_map/psum | solution.py:104
  101.1 3.4 %copy-start.1 = (f32[16,16,64,64]{3,2,1,0:T(8,128)}, f32[16,16,64,64]{3,2,1,0:T(8,128)S(1)}, u32[]{:S(2)}) copy-start(f32[16,16,64,64]{3,2,1,0:T(8,128)S(1)} %multiply_add_fusion) | copy-start | bytes 12582916
  104.5 7.0 %copy-start.8 = (f32[16,64]{1,0:T(8,128)S(1)}, f32[16,64]{1,0:T(8,128)}, u32[]{:S(2)}) copy-start(f32[16,64]{1,0:T(8,128)} %param.42) | copy-start | bytes 12292
  104.5 38.8 %copy-start.5 = (bf16[1024,256]{1,0:T(8,128)(2,1)S(1)}, bf16[1024,256]{1,0:T(8,128)(2,1)}, u32[]{:S(2)}) copy-start(bf16[1024,256]{1,0:T(8,128)(2,1)} %param.34) | copy-start | bytes 1572868
  104.5 45.1 %copy-start.14 = (bf16[16,2]{0,1:T(2,128)(2,1)S(1)}, bf16[16,2]{0,1:T(2,128)(2,1)}, u32[]{:S(2)}) copy-start(bf16[16,2]{0,1:T(2,128)(2,1)} %param.28) | copy-start | bytes 196
  104.5 66.0 %copy-start.13 = (s32[16,2]{0,1:T(2,128)S(1)}, s32[16,2]{0,1:T(2,128)}, u32[]{:S(2)}) copy-start(s32[16,2]{0,1:T(2,128)} %param.27) | copy-start | bytes 388
  104.5 82.6 %copy-start.12 = (bf16[2048]{0:T(1024)(128)(2,1)S(1)}, bf16[2048]{0:T(1024)(128)(2,1)}, u32[]{:S(2)}) copy-start(bf16[2048]{0:T(1024)(128)(2,1)} %param.49) | copy-start | bytes 12292
  104.5 84.6 %copy-start.4 = (bf16[16,2048]{1,0:T(8,128)(2,1)S(1)}, bf16[16,2048]{1,0:T(8,128)(2,1)}, u32[]{:S(2)}) copy-start(bf16[16,2048]{1,0:T(8,128)(2,1)} %param.25) | copy-start | bytes 196612
  104.5 84.7 %copy-start.9 = (f32[2048]{0:T(1024)S(1)}, f32[2048]{0:T(1024)}, u32[]{:S(2)}) copy-start(f32[2048]{0:T(1024)} %param.30) | copy-start | bytes 24580
  144.1 43.0 %all-to-all-start.1 = ((bf16[8,16,256]{2,1,0:T(8,128)(2,1)}), bf16[8,16,256]{2,1,0:T(8,128)(2,1)S(1)}, u32[]{:S(2)}, u32[]{:S(2)}) async-start(bf16[8,16,256]{2,1,0:T(8,128)(2,1)} %bitcast.12), calls=%async_computation.1 | async-start | bytes 131072 | tf_op jit(solution)/shard_map/all_to_all | solution.py:139
  149.6 147.5 %reduce-scatter.2.cloned.1.call-start = ((), (), s32[]{:S(2)}) async-start(), calls=%async_computation.4 | async-start | bytes 1114112 | tf_op jit(solution)/shard_map/reduce_scatter | solution.py:163
  220.7 5.3 %copy-start.2 = (bf16[2048,352]{0,1:T(8,128)(2,1)S(1)}, bf16[2048,352]{0,1:T(8,128)(2,1)}, u32[]{:S(2)}) copy-start(bf16[2048,352]{0,1:T(8,128)(2,1)} %param.46) | copy-start | bytes 4325380
  227.4 9.1 %copy-start.3 = (bf16[2048,352]{0,1:T(8,128)(2,1)S(1)}, bf16[2048,352]{0,1:T(8,128)(2,1)}, u32[]{:S(2)}) copy-start(bf16[2048,352]{0,1:T(8,128)(2,1)} %param.47) | copy-start | bytes 4325380
Sparse Core Ops, SparseCore 0:
  59.3 16.3 all-reduce.1
  240.4 56.5 reduce-scatter.1
